TPU v7x, 256 devices: a whole 4x4x8 slice. The times are simulated.
256 devices in a mesh: kv: 32 (over z, y), tp: 8 (over x, core).
Axes of the slice: x: 4, y: 4, z: 8, core: 2. Of those that a mesh axis runs over, the one named last changes fastest.
Arguments:
- tokens: bfloat16 [16, 4096], P(None, ('kv', 'tp')), may hold values from -17 to 17
- first_gain: float32 [4096], P('kv'), may hold values from 0.1 to 1.9
- first_gate: bfloat16 [4096, 11264], P('kv', 'tp'), may hold values from -0.09375 to 0.09375
- first_up: bfloat16 [4096, 11264], P('kv', 'tp'), may hold values from -0.09375 to 0.09375
- first_down: bfloat16 [11264, 4096], P('tp', 'kv'), may hold values from -0.0546875 to 0.0546875
- mixer_gain: float32 [4096], P('kv'), may hold values from 0.1 to 1.9
- w_query: bfloat16 [4096, 4096], P('kv', 'tp'), may hold values from -0.09375 to 0.09375
- w_key: bfloat16 [4096, 4096], P('kv', 'tp'), may hold values from -0.328125 to 0.328125
- w_value: bfloat16 [4096, 4096], P('kv', 'tp'), may hold values from -0.09375 to 0.09375
- w_output: bfloat16 [4096, 4096], P('tp', 'kv'), may hold values from -0.09375 to 0.09375
- lam_heads: float32 [32], P('tp'), may hold values from 0.3 to 0.8
- head_gain: float32 [128], replicated, may hold values from 0.1 to 1.9
- key_cache: bfloat16 [16, 8192, 32, 128], P(None, 'kv', 'tp'), may hold values from -1000 to 1000
- value_cache: bfloat16 [16, 8192, 32, 128], P(None, 'kv', 'tp'), may hold values from -6 to 6
- lengths: int32 [16], replicated, may hold values from 1 to 8192, 49152 in all
- last_gain: float32 [4096], P('kv'), may hold values from 0.1 to 1.9
- last_gate: bfloat16 [4096, 11264], P('kv', 'tp'), may hold values from -0.09375 to 0.09375
- last_up: bfloat16 [4096, 11264], P('kv', 'tp'), may hold values from -0.09375 to 0.09375
- last_down: bfloat16 [11264, 4096], P('tp', 'kv'), may hold values from -0.0546875 to 0.0546875
Outputs:
- result: bfloat16 [16, 4096], P(None, ('kv', 'tp'))
Inputs may be any that keep to these rules, and one draw needn't show every extreme that they name: Sequence b reads cached positions 0 to lengths[b] - 1 and its new token.
All inputs are finite; a program needn't handle non-finite values.
Results may differ from a plain program's by a relative error of at most 0.04.
Values may be sent and summed in bfloat16 or wider, within the bound.
No kernel may reach another device: no remote copies, remote signals or barrier semaphores. Data moves between devices by JAX's collectives and lax.ppermute only.
A program may use at most 64 MiB of HBM per device.

v0:
```python
import functools

import jax
import jax.numpy as jnp
from jax import lax
from jax.sharding import Mesh
from jax.sharding import PartitionSpec as P

WIDTH = 4096
HEAD_DIM = 64
VAL_DIM = 128
KV = ("kv_0", "kv_1")
KV_TP = ("kv_0", "kv_1", "tp")


epsilon = 1e-06
neg_fill = -1e30


def sent_to_all(array, axis):
    copies = jnp.broadcast_to(array, (lax.axis_size(axis), *array.shape))
    return lax.all_to_all(copies, axis, split_axis=0, concat_axis=0, tiled=True)


def laid_out(tiles, dim):
    tiles = jnp.moveaxis(tiles, 0, dim)
    shape = tiles.shape
    return tiles.reshape(*shape[:dim], shape[dim] * shape[dim + 1], *shape[dim + 2 :])


def gather_directly(array, axis, dim):
    tiles = sent_to_all(array, axis)
    return laid_out(tiles, dim)


def one_axis_at_a_time(array, axes):
    return functools.reduce(lax.psum, axes, array)


def in_blocks(array, dim, devices):
    shape = array.shape
    tiles = array.reshape(*shape[:dim], devices, shape[dim] // devices, *shape[dim + 1 :])
    return jnp.moveaxis(tiles, dim, 0)


def sent_and_summed(array, axis, dim):
    tiles = in_blocks(array, dim, lax.axis_size(axis))
    arrived = lax.all_to_all(tiles, axis, split_axis=0, concat_axis=0, tiled=True)
    return arrived.sum(axis=0)


def of_everyone(array, axis):
    return sent_to_all(array, axis).astype(jnp.float32).sum(axis=0)


def all_in_one(array, axis):
    leaves = jax.tree.leaves(array)
    turns = sorted(range(len(leaves)), key=lambda k: -leaves[k].size)
    width = (1, *leaves[turns[0]].shape)[-1]
    lines = [
        jnp.pad(leaves[k].reshape(-1), (0, -leaves[k].size % width)).reshape(-1, width)
        for k in turns
    ]
    both, at, found = (lax.all_gather(jnp.concatenate(lines), axis), 0, {})
    for k, line in zip(turns, lines):
        section = both[:, at : at + len(line)].reshape(len(both), -1)
        found[k] = section[:, : leaves[k].size].reshape(-1, *leaves[k].shape)
        at += len(line)
    numbers = iter(range(len(leaves)))
    return jax.tree.map(lambda _: found[next(numbers)], array)


def combined_by_axis(array, axes, combine):
    for axis in axes:
        pieces = all_in_one(
            jax.tree.map(
                lambda part, kind: part.astype(kind),
                array,
                (jnp.bfloat16, jnp.bfloat16, jnp.bfloat16),
            ),
            axis,
        )
        widened = [
            jax.tree.map(lambda part, own: part[k].astype(own.dtype), pieces, array)
            for k in range(lax.axis_size(axis))
        ]
        array = widened[0]
        for received in widened[1:]:
            array = combine(array, received)
    return array


def norm_block(stream_cols, gain):
    gathered = gather_directly(stream_cols, "tp", 1)
    wide = gathered.astype(jnp.float32)
    squares = jnp.sum(wide * wide, axis=1, keepdims=True)
    scaled = (wide * gain).astype(jnp.bfloat16)
    return (squares, scaled)


def gated_units(stream_cols, gain, gate_w, up_w, down_w):
    squares, scaled = norm_block(stream_cols, gain)
    part_gate = jnp.dot(scaled, gate_w, preferred_element_type=jnp.float32)
    part_up = jnp.dot(scaled, up_w, preferred_element_type=jnp.float32)
    gate_sum, up_sum, total_sq = (
        one_axis_at_a_time(part_gate.astype(jnp.bfloat16), KV).astype(jnp.float32),
        one_axis_at_a_time(part_up.astype(jnp.bfloat16), KV).astype(jnp.float32),
        one_axis_at_a_time(squares.astype(jnp.bfloat16), KV).astype(jnp.float32),
    )
    inv_rms = lax.rsqrt(total_sq / WIDTH + epsilon)
    hidden_act = (jax.nn.silu(gate_sum * inv_rms) * (up_sum * inv_rms)).astype(jnp.bfloat16)
    part_down = jnp.dot(hidden_act, down_w, preferred_element_type=jnp.float32)
    return sent_and_summed(part_down, "tp", 1)


def merge_parts(earlier, later):
    peak_one, sum_one, acc_one = earlier
    peak_two, sum_two, acc_two = later
    highest = jnp.maximum(peak_one, peak_two)
    scale_one = jnp.exp(peak_one - highest)
    scale_two = jnp.exp(peak_two - highest)
    return (
        highest,
        scale_one * sum_one + scale_two * sum_two,
        scale_one[..., None] * acc_one + scale_two[..., None] * acc_two,
    )


def attend(
    stream_cols,
    mixer_gain,
    w_query,
    w_key,
    w_value,
    w_output,
    lam_heads,
    head_gain,
    key_cache,
    value_cache,
    lengths,
):
    squares, scaled = norm_block(stream_cols, mixer_gain)
    part_query = jnp.dot(scaled, w_query, preferred_element_type=jnp.float32)
    part_key = jnp.dot(scaled, w_key, preferred_element_type=jnp.float32)
    part_value = jnp.dot(scaled, w_value, preferred_element_type=jnp.float32)
    query_sum, key_sum, value_sum, total_sq = (
        of_everyone(part_query.astype(jnp.bfloat16), KV).astype(jnp.float32),
        of_everyone(part_key.astype(jnp.bfloat16), KV).astype(jnp.float32),
        of_everyone(part_value.astype(jnp.bfloat16), KV).astype(jnp.float32),
        of_everyone(squares.astype(jnp.bfloat16), KV).astype(jnp.float32),
    )
    inv_rms = lax.rsqrt(total_sq / WIDTH + epsilon)
    rows_count = scaled.shape[0]
    shard_heads = key_cache.shape[2]
    local_pos = key_cache.shape[1]
    logit_scale = HEAD_DIM ** (-0.5)
    query_rows = (
        (query_sum * inv_rms).astype(jnp.bfloat16).reshape(rows_count, shard_heads, 2, HEAD_DIM)
    )
    fresh_key = (
        (key_sum * inv_rms).astype(jnp.bfloat16).reshape(rows_count, shard_heads, 2, HEAD_DIM)
    )
    new_value = (value_sum * inv_rms).astype(jnp.bfloat16).reshape(rows_count, shard_heads, VAL_DIM)
    offset = lax.axis_index(KV) * local_pos
    positions = offset + jnp.arange(local_pos, dtype=jnp.int32)
    live_mask = (positions[None, :] < lengths[:, None])[:, None, None, :]
    key_entries = key_cache.reshape(rows_count, local_pos, shard_heads, 2, HEAD_DIM)
    score_matrix = (
        jnp.einsum("bhmd,bphmd->bhmp", query_rows, key_entries, preferred_element_type=jnp.float32)
        * logit_scale
    )
    score_matrix = jnp.where(live_mask, score_matrix, neg_fill)
    peak_score = jnp.max(score_matrix, axis=-1)
    weights = jnp.where(live_mask, jnp.exp(score_matrix - peak_score[..., None]), 0.0)
    totals = jnp.sum(weights, axis=-1)
    weighted = jnp.einsum(
        "bhmp,bphe->bhme",
        weights.astype(jnp.bfloat16),
        value_cache,
        preferred_element_type=jnp.float32,
    )
    peak_score, totals, weighted = combined_by_axis((peak_score, totals, weighted), KV, merge_parts)
    self_score = (
        jnp.sum(query_rows.astype(jnp.float32) * fresh_key.astype(jnp.float32), axis=-1)
        * logit_scale
    )
    highest = jnp.maximum(peak_score, self_score)
    scale_old = jnp.exp(peak_score - highest)
    own_weight = jnp.exp(self_score - highest)
    own_round = lax.optimization_barrier(own_weight.astype(jnp.bfloat16)).astype(jnp.float32)
    totals = scale_old * totals + own_weight
    weighted = (
        scale_old[..., None] * weighted
        + own_round[..., None] * new_value.astype(jnp.float32)[:, :, None, :]
    )
    mixed = (
        weighted[:, :, 0] / totals[:, :, 0, None]
        - lam_heads[None, :, None] * weighted[:, :, 1] / totals[:, :, 1, None]
    )
    normed = (
        mixed * lax.rsqrt(jnp.mean(mixed * mixed, axis=-1, keepdims=True) + epsilon) * head_gain
    )
    attended = normed.astype(jnp.bfloat16).reshape(rows_count, shard_heads * VAL_DIM)
    part_out = jnp.dot(attended, w_output, preferred_element_type=jnp.float32)
    return sent_and_summed(part_out, "tp", 1)


def on_device(
    tokens,
    first_gain,
    first_gate,
    first_up,
    first_down,
    mixer_gain,
    w_query,
    w_key,
    w_value,
    w_output,
    lam_heads,
    head_gain,
    key_cache,
    value_cache,
    lengths,
    last_gain,
    last_gate,
    last_up,
    last_down,
):
    first_branch = gated_units(tokens, first_gain, first_gate, first_up, first_down)
    first = (tokens.astype(jnp.float32) + 0.5 * first_branch).astype(jnp.bfloat16)
    projected = attend(
        first,
        mixer_gain,
        w_query,
        w_key,
        w_value,
        w_output,
        lam_heads,
        head_gain,
        key_cache,
        value_cache,
        lengths,
    )
    second = (first.astype(jnp.float32) + projected).astype(jnp.bfloat16)
    last_branch = gated_units(second, last_gain, last_gate, last_up, last_down)
    return (second.astype(jnp.float32) + 0.5 * last_branch).astype(jnp.bfloat16)


def solution(mesh):
    finer = Mesh(mesh.devices.reshape(8, 4, mesh.shape["tp"]), ("kv_0", "kv_1", "tp"))
    return jax.shard_map(
        on_device,
        mesh=finer,
        in_specs=(
            P(None, KV_TP),
            P(KV),
            P(KV, "tp"),
            P(KV, "tp"),
            P("tp", KV),
            P(KV),
            P(KV, "tp"),
            P(KV, "tp"),
            P(KV, "tp"),
            P("tp", KV),
            P("tp"),
            P(),
            P(None, KV, "tp", None),
            P(None, KV, "tp", None),
            P(),
            P(KV),
            P(KV, "tp"),
            P(KV, "tp"),
            P("tp", KV),
        ),
        out_specs=P(None, KV_TP),
        check_vma=False,
    )
```

profile of v0, /device:TPU:1, one launch (start us, length us, event | category | flops | bytes accessed | tf_op | source)
XLA Modules:
  0.0 436.8 jit_solution(5309866430094227475)
XLA Ops:
  6.5 0.7 broadcast_in_dim.32
  7.4 10.2 %all_to_all.50 = bf16[8,2,128]{2,1,0:T(2,128)(2,1)S(1)} all-to-all(bf16[8,2,128]{2,1,0:T(2,128)(2,1)S(1)} %reshape.1266), channel_id=1, replica_groups=mesh['kv_0'=8,'kv_1'=4,'tp'=8] {'tp'}, dimensions={0} | all-to-all | bytes 8192 | tf_op jit(solution)/shard_map/all_to_all | solution.py:22
  17.7 0.6 fusion.6
  18.4 1.4 convolution_convert_fusion.2
  19.8 1.8 convolution_convert_fusion.3
  21.7 68.7 %all-reduce.11.cloned.1.call-done = (bf16[16,1408]{1,0:T(8,128)(2,1)}, bf16[16,1408]{1,0:T(8,128)(2,1)}, bf16[16,1]{0,1:T(2,128)(2,1)}) async-done(((bf16[16,1408]{1,0:T(8,128)(2,1)}, bf16[16,1408]{1,0:T(8,128)(2,1)}, bf16[16,1]{0,1:T(2,128)(2,1)}), (bf16[16,1408]{1,0:T(8,128)(2,1)}, bf16[16,1408]{1,0:T(8,128)(2,1)}, bf16[16,1]{0,1:T(2,128)(2,1)})) %all-reduce.11.cloned.1.call-update) | async-done | bytes 90160 | tf_op jit(solution)/shard_map/psum | solution.py:37
  90.4 50.1 %all-reduce.15.cloned.1.call-done = (bf16[16,1408]{1,0:T(8,128)(2,1)}, bf16[16,1408]{1,0:T(8,128)(2,1)}, bf16[16,1]{0,1:T(2,128)(2,1)}) async-done(((bf16[16,1408]{1,0:T(8,128)(2,1)}, bf16[16,1408]{1,0:T(8,128)(2,1)}, bf16[16,1]{0,1:T(2,128)(2,1)}), (bf16[16,1408]{1,0:T(8,128)(2,1)}, bf16[16,1408]{1,0:T(8,128)(2,1)}, bf16[16,1]{0,1:T(2,128)(2,1)})) %all-reduce.15.cloned.1.call-update) | async-done | bytes 90160 | tf_op jit(solution)/shard_map/psum | solution.py:37
  140.5 0.6 rsqrt_bitcast_fusion.1
  141.2 1.3 fusion.35
  142.7 11.5 %all_to_all.51 = f32[8,1,256]{2,1,0:T(1,128)S(1)} all-to-all(f32[8,1,256]{2,1,0:T(1,128)S(1)} %reshape.1268), channel_id=1, replica_groups=mesh['kv_0'=8,'kv_1'=4,'tp'=8] {'tp'}, dimensions={0} | all-to-all | bytes 16384 | tf_op jit(solution)/shard_map/all_to_all | solution.py:48
  154.1 0.5 broadcast.199
  154.6 0.7 reduce.39
  155.4 0.7 add_convert_fusion.2
  156.2 7.6 %all_to_all.52 = bf16[8,2,128]{2,1,0:T(2,128)(2,1)S(1)} all-to-all(bf16[8,2,128]{2,1,0:T(2,128)(2,1)S(1)} %reshape.1270), channel_id=1, replica_groups=mesh['kv_0'=8,'kv_1'=4,'tp'=8] {'tp'}, dimensions={0} | all-to-all | bytes 8192 | tf_op jit(solution)/shard_map/all_to_all | solution.py:22
  164.2 0.6 broadcast_in_dim.36
  164.8 8.1 %all-to-all-start.4 = ((bf16[32,16,1]{1,2,0:T(2,128)(2,1)}), bf16[32,16,1]{1,2,0:T(2,128)(2,1)S(1)}, u32[]{:S(2)}, u32[]{:S(2)}) async-start(bf16[32,16,1]{1,2,0:T(2,128)(2,1)} %broadcast_in_dim.36), calls=%async_computation.4 | async-start | bytes 32768 | tf_op jit(solution)/shard_map/all_to_all | solution.py:22
  172.9 0.7 multiply_convert_fusion.7
  173.6 1.0 convolution_convert_fusion.6
  174.6 6.9 %all-to-all-done.4 = bf16[32,16,1]{1,2,0:T(2,128)(2,1)S(1)} async-done(((bf16[32,16,1]{1,2,0:T(2,128)(2,1)}), bf16[32,16,1]{1,2,0:T(2,128)(2,1)S(1)}, u32[]{:S(2)}, u32[]{:S(2)}) %all-to-all-start.4) | async-done | bytes 1056 | tf_op jit(solution)/shard_map/all_to_all | solution.py:22
  181.6 0.9 broadcast_in_dim.35
  182.4 3.9 all-to-all-start.3
  186.4 7.4 %copy.85 = bf16[16,256,4,128]{1,3,2,0:T(8,128)(2,1)} copy(bf16[16,256,4,128]{3,2,1,0:T(4,128)(2,1)} %param.31) | data formatting | bytes 8388608 | tf_op args[12]
  194.0 7.3 %all-to-all-done.3 = bf16[32,16,512]{2,1,0:T(8,128)(2,1)S(1)} async-done(((bf16[32,16,512]{2,1,0:T(8,128)(2,1)}), bf16[32,16,512]{2,1,0:T(8,128)(2,1)S(1)}, u32[]{:S(2)}, u32[]{:S(2)}) %all-to-all-start.3) | async-done | bytes 524320 | tf_op jit(solution)/shard_map/all_to_all | solution.py:22
  201.3 0.9 broadcast_in_dim.39
  202.2 6.2 %all-to-all-start.5 = ((bf16[32,16,512]{2,1,0:T(8,128)(2,1)}), bf16[32,16,512]{2,1,0:T(8,128)(2,1)S(1)}, u32[]{:S(2)}, u32[]{:S(2)}) async-start(bf16[32,16,512]{2,1,0:T(8,128)(2,1)} %broadcast_in_dim.39), calls=%async_computation.5 | async-start | bytes 1048576 | tf_op jit(solution)/shard_map/all_to_all | solution.py:22
  208.9 14.5 %all-to-all-done.5 = bf16[32,16,512]{2,1,0:T(8,128)(2,1)S(1)} async-done(((bf16[32,16,512]{2,1,0:T(8,128)(2,1)}), bf16[32,16,512]{2,1,0:T(8,128)(2,1)S(1)}, u32[]{:S(2)}, u32[]{:S(2)}) %all-to-all-start.5) | async-done | bytes 524320 | tf_op jit(solution)/shard_map/all_to_all | solution.py:22
  223.4 0.9 broadcast_in_dim.40
  224.2 6.3 %all-to-all-start.6 = ((bf16[32,16,512]{2,1,0:T(8,128)(2,1)}), bf16[32,16,512]{2,1,0:T(8,128)(2,1)S(1)}, u32[]{:S(2)}, u32[]{:S(2)}) async-start(bf16[32,16,512]{2,1,0:T(8,128)(2,1)} %broadcast_in_dim.40), calls=%async_computation.6 | async-start | bytes 1048576 | tf_op jit(solution)/shard_map/all_to_all | solution.py:22
  231.0 3.0 fusion.30
  234.2 0.3 fusion.105
  234.6 0.7 fusion.2
  235.6 22.2 %all-gather.2 = bf16[8,130,128]{2,1,0:T(8,128)(2,1)S(1)} all-gather(bf16[1,130,128]{2,1,0:T(8,128)(2,1)S(1)} %maximum_bitcast_fusion), channel_id=2, replica_groups=mesh['kv_0'=8,'kv_1'=4,'tp'=8] {'kv_0'}, dimensions={0}, use_global_device_ids=true | all-gather | bytes 299520 | tf_op jit(solution)/shard_map/all_gather | solution.py:64
  257.9 0.3 fusion.17
  258.2 9.5 %all-gather.3 = bf16[4,130,128]{2,1,0:T(8,128)(2,1)S(1)} all-gather(bf16[1,130,128]{2,1,0:T(8,128)(2,1)S(1)} %maximum_bitcast_fusion.1), channel_id=3, replica_groups=mesh['kv_0'=8,'kv_1'=4,'tp'=8] {'kv_1'}, dimensions={0}, use_global_device_ids=true | all-gather | bytes 166400 | tf_op jit(solution)/shard_map/all_gather | solution.py:64
  271.1 0.6 fusion.11
  272.7 17.1 %all_to_all.53 = f32[8,1,256]{2,1,0:T(1,128)S(1)} all-to-all(f32[8,1,256]{2,1,0:T(1,128)S(1)} %reshape.1272), channel_id=1, replica_groups=mesh['kv_0'=8,'kv_1'=4,'tp'=8] {'tp'}, dimensions={0} | all-to-all | bytes 16384 | tf_op jit(solution)/shard_map/all_to_all | solution.py:48
  289.8 0.7 reduce.40
  290.7 7.6 %all_to_all.54 = bf16[8,2,128]{2,1,0:T(2,128)(2,1)S(1)} all-to-all(bf16[8,2,128]{2,1,0:T(2,128)(2,1)S(1)} %reshape.1274), channel_id=1, replica_groups=mesh['kv_0'=8,'kv_1'=4,'tp'=8] {'tp'}, dimensions={0} | all-to-all | bytes 8192 | tf_op jit(solution)/shard_map/all_to_all | solution.py:22
  298.4 0.7 fusion.8
  299.2 0.8 convolution_convert_fusion
  300.0 0.8 convolution_convert_fusion.1
  300.8 64.7 %all-reduce.9.cloned.1.call-done = (bf16[16,1408]{1,0:T(8,128)(2,1)}, bf16[16,1408]{1,0:T(8,128)(2,1)}, bf16[16,1]{0,1:T(2,128)(2,1)}) async-done(((bf16[16,1408]{1,0:T(8,128)(2,1)}, bf16[16,1408]{1,0:T(8,128)(2,1)}, bf16[16,1]{0,1:T(2,128)(2,1)}), (bf16[16,1408]{1,0:T(8,128)(2,1)}, bf16[16,1408]{1,0:T(8,128)(2,1)}, bf16[16,1]{0,1:T(2,128)(2,1)})) %all-reduce.9.cloned.1.call-update) | async-done | bytes 90160 | tf_op jit(solution)/shard_map/psum | solution.py:37
  365.6 50.0 %all-reduce.13.cloned.1.call-done = (bf16[16,1408]{1,0:T(8,128)(2,1)}, bf16[16,1408]{1,0:T(8,128)(2,1)}, bf16[16,1]{0,1:T(2,128)(2,1)}) async-done(((bf16[16,1408]{1,0:T(8,128)(2,1)}, bf16[16,1408]{1,0:T(8,128)(2,1)}, bf16[16,1]{0,1:T(2,128)(2,1)}), (bf16[16,1408]{1,0:T(8,128)(2,1)}, bf16[16,1408]{1,0:T(8,128)(2,1)}, bf16[16,1]{0,1:T(2,128)(2,1)})) %all-reduce.13.cloned.1.call-update) | async-done | bytes 90160 | tf_op jit(solution)/shard_map/psum | solution.py:37
  415.6 0.6 rsqrt_bitcast_fusion
  416.2 1.0 fusion.36
  417.5 11.5 %all_to_all.55 = f32[8,1,256]{2,1,0:T(1,128)S(1)} all-to-all(f32[8,1,256]{2,1,0:T(1,128)S(1)} %reshape.1276), channel_id=1, replica_groups=mesh['kv_0'=8,'kv_1'=4,'tp'=8] {'tp'}, dimensions={0} | all-to-all | bytes 16384 | tf_op jit(solution)/shard_map/all_to_all | solution.py:48
  428.9 0.7 reduce.41
  429.7 0.6 add_convert_fusion
  (127 shorter events, 7.8 us)
Async XLA Ops:
  6.5 11.9 %copy-start = (bf16[128,1408]{1,0:T(8,128)(2,1)S(1)}, bf16[128,1408]{1,0:T(8,128)(2,1)}, u32[]{:S(2)}) copy-start(bf16[128,1408]{1,0:T(8,128)(2,1)} %param.22) | copy-start | bytes 1081348
  6.5 83.9 %all-reduce.11.cloned.1.call-start = ((), (), s32[]{:S(2)}) async-start(), calls=%async_computation.11 | async-start | bytes 181248 | tf_op jit(solution)/shard_map/psum | solution.py:37
  21.7 118.9 %all-reduce.15.cloned.1.call-start = ((), (), s32[]{:S(2)}) async-start(), calls=%async_computation.13 | async-start | bytes 181248 | tf_op jit(solution)/shard_map/psum | solution.py:37
  164.8 16.8 %all-to-all-start.4 = ((bf16[32,16,1]{1,2,0:T(2,128)(2,1)}), bf16[32,16,1]{1,2,0:T(2,128)(2,1)S(1)}, u32[]{:S(2)}, u32[]{:S(2)}) async-start(bf16[32,16,1]{1,2,0:T(2,128)(2,1)} %broadcast_in_dim.36), calls=%async_computation.4 | async-start | bytes 32768 | tf_op jit(solution)/shard_map/all_to_all | solution.py:22
  182.4 18.9 %all-to-all-start.3 = ((bf16[32,16,512]{2,1,0:T(8,128)(2,1)}), bf16[32,16,512]{2,1,0:T(8,128)(2,1)S(1)}, u32[]{:S(2)}, u32[]{:S(2)}) async-start(bf16[32,16,512]{2,1,0:T(8,128)(2,1)} %broadcast_in_dim.35), calls=%async_computation.3 | async-start | bytes 1048576 | tf_op jit(solution)/shard_map/all_to_all | solution.py:22
  186.3 7.5 %copy-start.5 = (bf16[512,128]{1,0:T(8,128)(2,1)S(1)}, bf16[512,128]{1,0:T(8,128)(2,1)}, u32[]{:S(2)}) copy-start(bf16[512,128]{1,0:T(8,128)(2,1)} %param.28) | copy-start | bytes 393220
  186.3 7.6 %copy-start.3 = (bf16[128,512]{1,0:T(8,128)(2,1)S(1)}, bf16[128,512]{1,0:T(8,128)(2,1)}, u32[]{:S(2)}) copy-start(bf16[128,512]{1,0:T(8,128)(2,1)} %param.26) | copy-start | bytes 393220
  186.3 22.1 %copy-start.9 = (s32[16]{0:T(128)S(1)}, s32[16]{0:T(128)}, u32[]{:S(2)}) copy-start(s32[16]{0:T(128)} %param.33) | copy-start | bytes 196
  186.3 22.2 %copy-start.4 = (bf16[128,512]{1,0:T(8,128)(2,1)S(1)}, bf16[128,512]{1,0:T(8,128)(2,1)}, u32[]{:S(2)}) copy-start(bf16[128,512]{1,0:T(8,128)(2,1)} %param.27) | copy-start | bytes 393220
  202.2 21.2 %all-to-all-start.5 = ((bf16[32,16,512]{2,1,0:T(8,128)(2,1)}), bf16[32,16,512]{2,1,0:T(8,128)(2,1)S(1)}, u32[]{:S(2)}, u32[]{:S(2)}) async-start(bf16[32,16,512]{2,1,0:T(8,128)(2,1)} %broadcast_in_dim.39), calls=%async_computation.5 | async-start | bytes 1048576 | tf_op jit(solution)/shard_map/all_to_all | solution.py:22
  224.2 46.7 %all-to-all-start.6 = ((bf16[32,16,512]{2,1,0:T(8,128)(2,1)}), bf16[32,16,512]{2,1,0:T(8,128)(2,1)S(1)}, u32[]{:S(2)}, u32[]{:S(2)}) async-start(bf16[32,16,512]{2,1,0:T(8,128)(2,1)} %broadcast_in_dim.40), calls=%async_computation.6 | async-start | bytes 1048576 | tf_op jit(solution)/shard_map/all_to_all | solution.py:22
  230.5 135.1 %all-reduce.9.cloned.1.call-start = ((), (), s32[]{:S(2)}) async-start(), calls=%async_computation.10 | async-start | bytes 181248 | tf_op jit(solution)/shard_map/psum | solution.py:37
  230.8 3.7 copy-start.10
  234.5 37.5 %copy-start.7 = (f32[4]{0:T(128)S(1)}, f32[4]{0:T(128)}, u32[]{:S(2)}) copy-start(f32[4]{0:T(128)} %param.29) | copy-start | bytes 52
  234.5 37.7 %copy-start.8 = (f32[128]{0:T(128)S(1)}, f32[128]{0:T(128)}, u32[]{:S(2)}) copy-start(f32[128]{0:T(128)} %param.30) | copy-start | bytes 1540
  234.6 64.6 %copy-start.1 = (bf16[128,1408]{1,0:T(8,128)(2,1)S(1)}, bf16[128,1408]{1,0:T(8,128)(2,1)}, u32[]{:S(2)}) copy-start(bf16[128,1408]{1,0:T(8,128)(2,1)} %param.36) | copy-start | bytes 1081348
  234.6 64.6 %copy-start.6 = (f32[128]{0:T(128)S(1)}, f32[128]{0:T(128)}, u32[]{:S(2)}) copy-start(f32[128]{0:T(128)} %param.34) | copy-start | bytes 1540
  234.6 65.4 %copy-start.2 = (bf16[128,1408]{1,0:T(8,128)(2,1)S(1)}, bf16[128,1408]{1,0:T(8,128)(2,1)}, u32[]{:S(2)}) copy-start(bf16[128,1408]{1,0:T(8,128)(2,1)} %param.35) | copy-start | bytes 1081348
  235.3 180.9 %copy-start.11 = (bf16[1408,128]{1,0:T(8,128)(2,1)S(1)}, bf16[1408,128]{1,0:T(8,128)(2,1)}, u32[]{:S(2)}) copy-start(bf16[1408,128]{1,0:T(8,128)(2,1)} %param.37) | copy-start | bytes 1081348
  300.8 114.8 %all-reduce.13.cloned.1.call-start = ((), (), s32[]{:S(2)}) async-start(), calls=%async_computation.12 | async-start | bytes 181248 | tf_op jit(solution)/shard_map/psum | solution.py:37
Sparse Core Ops, SparseCore 0:
  21.8 68.6 all-reduce.10
  92.9 47.5 all-reduce.14
  300.9 64.6 all-reduce.8
  367.9 47.5 all-reduce.12
where the time goes:
time: 438 us; the launch traced here: 437 us
  waiting for transfers between devices  262 us (60%)
  blocking collectives  97.2 us (22%)
  starting transfers between devices  24.7 us (6%)
  local copies, waits for them, and re-layouts  17.4 us (4%)
  between operations  13.7 us (3%)
  matrix products  12.4 us (3%)
  other arithmetic  9.27 us (2%)
    psum x4, waiting for transfers between devices, one_axis_at_a_time(): return functools.reduce(lax.psum, axes, array)  234 us
    all_to_all x3, blocking collectives, sent_and_summed(): lax.all_to_all(tiles, axis, split_axis=0, concat_axis=0, tiled=True)  40 us
    all_gather x2, blocking collectives, all_in_one(): both, at, found = (lax.all_gather(jnp.concatenate(lines), axis), 0, {})  31.7 us
    all_to_all x4, waiting for transfers between devices, sent_to_all(): return lax.all_to_all(copies, axis, split_axis=0, concat_axis=0, tiled=True)  28.7 us
    all_to_all x3, blocking collectives, sent_to_all(): return lax.all_to_all(copies, axis, split_axis=0, concat_axis=0, tiled=True)  25.5 us
    all_to_all x4, starting transfers between devices, sent_to_all(): return lax.all_to_all(copies, axis, split_axis=0, concat_axis=0, tiled=True)  24.5 us
  transfers between devices with their start and end apart: 8, of which 7 were waited for; matrix products, arithmetic and copies ran while one was open for 4% of the time, Pallas kernels for 0%

commit v1 on v0

v1 whole, which is shorter than its diff:
```python
import functools

import jax
import jax.numpy as jnp
from jax import lax
from jax.experimental import pallas as pl
from jax.experimental.pallas import tpu as pltpu
from jax.sharding import Mesh
from jax.sharding import PartitionSpec as P

WIDTH = 4096
ROWS = 16
HEAD_DIM = 64
LANES = 128
KV = ("kv_0", "kv_1")
KV_TP = ("kv_0", "kv_1", "tp")

epsilon = 1e-06
neg_fill = -1e30
f32 = jnp.float32
bf16 = jnp.bfloat16


def iota(shape, dim):
    return lax.broadcasted_iota(jnp.int32, shape, dim)


def matmul(a, b):
    return jnp.dot(a, b, preferred_element_type=f32)


def in_kernel(body, outs, *args, smem=(), vmem_limit=16 << 20):
    spaces = [pltpu.SMEM if k in smem else pltpu.VMEM for k in range(len(args))]
    return pl.pallas_call(
        body,
        out_shape=outs,
        in_specs=[pl.BlockSpec(memory_space=space) for space in spaces],
        out_specs=jax.tree.map(lambda _: pl.BlockSpec(memory_space=pltpu.VMEM), outs),
        compiler_params=pltpu.CompilerParams(vmem_limit_bytes=vmem_limit),
        name=body.__name__,
    )(*args)


def swap(blocks, axis):
    return lax.all_to_all(blocks, axis, split_axis=0, concat_axis=0, tiled=True)


def like(shape, kind):
    return jax.ShapeDtypeStruct(shape, kind)


def kv_index():
    return lax.axis_index("kv_0") * lax.axis_size("kv_1") + lax.axis_index("kv_1")


def halves(column):
    high = column.astype(bf16)
    low = (column - high.astype(f32)).astype(bf16)
    return high.astype(f32), low.astype(f32)


def thirds(column):
    high, low = halves(column)
    rest = (column - high) - low
    return high, low, rest


def own_columns(shape_dim):
    place = lax.axis_index("tp") * ROWS
    return (iota((ROWS, LANES), 1) == iota((ROWS, LANES), 0) + place).astype(bf16)


def spread_tokens(tokens_ref, out_ref):
    block = matmul(tokens_ref[...], own_columns(0)).astype(bf16)
    out_ref[...] = jnp.broadcast_to(block[None], out_ref.shape)


def send_units(stream, gain_ref, gate_ref, up_ref, out_ref):
    wide = stream.astype(f32)
    high, low = halves(jnp.sum(wide * wide, axis=1, keepdims=True))
    scaled = (wide * gain_ref[...]).astype(bf16)
    lane = iota((ROWS, LANES), 1)
    squares = jnp.where(lane == 0, high, jnp.where(lane == 1, low, 0.0)).astype(bf16)
    gate = matmul(scaled, gate_ref[...]).astype(bf16)
    up = matmul(scaled, up_ref[...]).astype(bf16)
    tiles = gate.shape[1] // LANES
    for k in range(tiles):
        for half in range(2):
            rows = slice(half * 8, half * 8 + 8)
            cols = slice(k * LANES, (k + 1) * LANES)
            out_ref[2 * k + half, 0:8] = gate[rows, cols]
            out_ref[2 * k + half, 8:16] = up[rows, cols]
            out_ref[2 * k + half, 16:24] = squares[rows]
    spare = out_ref.shape[0] - 2 * tiles
    out_ref[2 * tiles :] = jnp.zeros((spare, 24, LANES), bf16)


def first_units(blocks_ref, gain_ref, gate_ref, up_ref, out_ref, stream_ref):
    stream = jnp.sum(blocks_ref[...].astype(f32), axis=0).astype(bf16)
    stream_ref[...] = stream
    send_units(stream, gain_ref, gate_ref, up_ref, out_ref)


def last_units(blocks_ref, before_ref, gain_ref, gate_ref, up_ref, out_ref, stream_ref):
    stream = (before_ref[...].astype(f32) + jnp.sum(blocks_ref[...], axis=0)).astype(bf16)
    stream_ref[...] = stream
    send_units(stream, gain_ref, gate_ref, up_ref, out_ref)


def gate_units(parts_ref, out_ref):
    total = jnp.sum(parts_ref[...].astype(f32), axis=0)
    squares = jnp.sum(total[16:24], axis=1, keepdims=True)
    inv_rms = lax.rsqrt(squares / WIDTH + epsilon)
    hidden = (jax.nn.silu(total[0:8] * inv_rms) * (total[8:16] * inv_rms)).astype(bf16)
    out_ref[...] = jnp.broadcast_to(hidden[None], out_ref.shape)


def sum_down(hidden_ref, down_ref, out_ref):
    tiles = down_ref.shape[0] // LANES
    hidden = jnp.concatenate(
        [
            jnp.concatenate([hidden_ref[2 * k], hidden_ref[2 * k + 1]], axis=0)
            for k in range(tiles)
        ],
        axis=1,
    )
    part = matmul(hidden, down_ref[...])
    out_ref[...] = jnp.broadcast_to(part[None], out_ref.shape)


def send_heads(
    blocks_ref, tokens_ref, gain_ref, query_ref, key_ref, value_ref, out_ref, stream_ref
):
    branch = jnp.sum(blocks_ref[...], axis=0)
    stream = (tokens_ref[...].astype(f32) + 0.5 * branch).astype(bf16)
    stream_ref[...] = stream
    wide = stream.astype(f32)
    high, low = halves(jnp.sum(wide * wide, axis=1, keepdims=True))
    lane = iota((8, LANES), 1)
    squares = jnp.where(lane == 0, high[0:8], jnp.where(lane == 1, low[0:8], 0.0))
    squares = jnp.where(lane == 2, high[8:16], jnp.where(lane == 3, low[8:16], squares))
    scaled = (wide * gain_ref[...]).astype(bf16)
    heads = query_ref.shape[1] // LANES

    def stacked(products):
        return [products[:, h * LANES : (h + 1) * LANES] for h in range(heads)]

    query = stacked(matmul(scaled, query_ref[...]).astype(bf16))
    key = stacked(matmul(scaled, key_ref[...]).astype(bf16))
    value = stacked(matmul(scaled, value_ref[...]).astype(bf16))
    fresh = jnp.concatenate(key + value, axis=0)
    row, col = iota((LANES, LANES), 0), iota((LANES, LANES), 1)
    order = (col == (row % 8) * ROWS + row // 8).astype(bf16)
    fresh = matmul(order, fresh).astype(bf16)
    devices = out_ref.shape[0]
    query = jnp.concatenate(query, axis=0)
    out_ref[:, 0:64] = jnp.broadcast_to(query[None], (devices, 64, LANES))
    out_ref[0:ROWS, 64:72] = fresh.reshape(ROWS, 8, LANES)
    out_ref[ROWS:, 64:72] = jnp.zeros((devices - ROWS, 8, LANES), bf16)
    out_ref[:, 72:80] = jnp.broadcast_to(squares.astype(bf16)[None], (devices, 8, LANES))


def attend(lengths_ref, parts_ref, keys_ref, values_ref, out_ref, own_ref, held_ref):
    total = jnp.sum(parts_ref[...].astype(f32), axis=0)
    squares = total[72:80]
    squares = jnp.concatenate(
        [
            jnp.sum(squares[:, 0:2], axis=1, keepdims=True),
            jnp.sum(squares[:, 2:4], axis=1, keepdims=True),
        ],
        axis=0,
    )
    inv_rms = lax.rsqrt(squares / WIDTH + epsilon)
    query = (total[0:64] * jnp.concatenate([inv_rms] * 4, axis=0)).astype(bf16)
    row, col = iota((LANES, 64), 0), iota((LANES, 64), 1)
    order = (col == (row % 8) // 2 * ROWS + row // 8).astype(bf16)
    query = matmul(order, query)
    row, lane = iota((LANES, LANES), 0), iota((LANES, LANES), 1)
    query = jnp.where(lane // HEAD_DIM == row % 2, query, 0.0)
    held_ref[...] = query
    place = kv_index()
    own = jnp.sum(jnp.where(iota((ROWS, 1), 0) == place, inv_rms, 0.0), axis=0, keepdims=True)
    own_ref[0:8] = (total[64:72] * own).astype(bf16).astype(f32)
    own_ref[8:16] = held_ref[pl.ds(pl.multiple_of(lax.rem(place, ROWS) * 8, 8), 8), :]
    query = query.astype(bf16)
    columns = keys_ref.shape[1]
    positions = columns // 4
    offset = place * positions
    col = iota((8, columns), 1)
    same_head = col % 4 == iota((8, columns), 0) // 2
    position = col // 4 + offset
    stat_lane = iota((8, LANES), 1)
    for b in range(ROWS):
        scores = (
            lax.dot_general(
                query[b * 8 : b * 8 + 8],
                keys_ref[b],
                (((1,), (1,)), ((), ())),
                preferred_element_type=f32,
            )
            * HEAD_DIM**-0.5
        )
        live = same_head & (position < lengths_ref[b])
        scores = jnp.where(live, scores, neg_fill)
        peak = jnp.max(scores, axis=1, keepdims=True)
        weights = jnp.where(live, jnp.exp(scores - peak), 0.0)
        amount = jnp.sum(weights, axis=1, keepdims=True)
        weighted = matmul(weights.astype(bf16), values_ref[b])
        stats = jnp.zeros((8, LANES), f32)
        for k, part in enumerate(thirds(peak) + thirds(amount)):
            stats = jnp.where(stat_lane == k, part, stats)
        out_ref[b, 0:8] = weighted.astype(bf16)
        out_ref[b, 8:16] = stats.astype(bf16)
    out_ref[ROWS:] = jnp.zeros((out_ref.shape[0] - ROWS, 16, LANES), bf16)


def merge(parts_ref, own_ref, lam_ref, gain_ref, out_ref):
    devices = parts_ref.shape[0]
    stats = parts_ref[:, 8:16].reshape(devices * 8, LANES)
    row, col = iota((LANES, 2 * LANES), 0), iota((LANES, 2 * LANES), 1)
    pick = (row // 3 == col // LANES).astype(bf16)
    stats = matmul(stats, pick)
    peaks = stats[:, 0:LANES].reshape(devices, 8, LANES)
    amounts = stats[:, LANES:].reshape(devices, 8, LANES)
    fresh = own_ref[0:8].astype(bf16)
    query = own_ref[8:16]
    row, col = iota((8, 8), 0), iota((8, 8), 1)
    key = matmul((col == row // 2).astype(bf16), fresh)
    value = matmul((col == row // 2 + 4).astype(bf16), fresh)
    self_score = jnp.sum(query * key, axis=1, keepdims=True) * HEAD_DIM**-0.5
    highest = jnp.maximum(jnp.max(peaks, axis=0), self_score)
    scale = jnp.exp(peaks - highest[None])
    own_weight = jnp.exp(self_score - highest)
    amount = jnp.sum(scale * amounts, axis=0) + own_weight
    weighted = jnp.sum(scale * parts_ref[:, 0:8].astype(f32), axis=0)
    weighted = weighted + own_weight.astype(bf16).astype(f32) * value
    ratio = weighted / amount
    row, lane = iota((8, 4), 0), iota((8, 4), 1)
    lam = jnp.sum(jnp.where(lane == row // 2, lam_ref[...], 0.0), axis=1, keepdims=True)
    row = iota((8, LANES), 0)
    ratio = jnp.where(row % 2 == 0, ratio, -lam * ratio)
    mixed = ratio + pltpu.roll(ratio, 7, 0)
    spread = jnp.mean(mixed * mixed, axis=1, keepdims=True)
    normed = mixed * lax.rsqrt(spread + epsilon) * gain_ref[...]
    attended = jnp.where(row % 2 == 0, normed, 0.0).astype(bf16)
    out_ref[...] = jnp.broadcast_to(attended[None], out_ref.shape)


def sum_heads(attended_ref, weight_ref, out_ref):
    rows = attended_ref[0:ROWS].reshape(LANES, LANES)
    row, col = iota((64, LANES), 0), iota((64, LANES), 1)
    order = (col == (row % ROWS) * 8 + row // ROWS * 2).astype(bf16)
    rows = matmul(order, rows).astype(bf16)
    attended = jnp.concatenate([rows[h * ROWS : (h + 1) * ROWS] for h in range(4)], axis=1)
    part = matmul(attended, weight_ref[...])
    out_ref[...] = jnp.broadcast_to(part[None], out_ref.shape)


def finish(blocks_ref, before_ref, out_ref):
    branch = jnp.sum(blocks_ref[...], axis=0)
    stream = (before_ref[...].astype(f32) + 0.5 * branch).astype(bf16)
    own = lax.dot_general(
        stream, own_columns(0), (((1,), (1,)), ((), ())), preferred_element_type=f32
    )
    out_ref[...] = own.astype(bf16)


def on_device(
    tokens,
    first_gain,
    first_gate,
    first_up,
    first_down,
    mixer_gain,
    w_query,
    w_key,
    w_value,
    w_output,
    lam_heads,
    head_gain,
    key_cache,
    value_cache,
    lengths,
    last_gain,
    last_gate,
    last_up,
    last_down,
):
    kv, tp = lax.axis_size(KV), lax.axis_size("tp")
    stream_like = like((ROWS, LANES), bf16)
    units_like = like((kv, 24, LANES), bf16)
    tile_like = like((kv, 8, LANES), bf16)
    sums_like = like((tp, ROWS, LANES), f32)

    def hidden_sums(units, down_w):
        hidden = in_kernel(gate_units, tile_like, swap(units, KV))
        return swap(in_kernel(sum_down, sums_like, swap(hidden, KV), down_w), "tp")

    blocks = swap(in_kernel(spread_tokens, like((tp, ROWS, LANES), bf16), tokens), "tp")
    units, stream = in_kernel(
        first_units,
        (units_like, stream_like),
        blocks,
        first_gain.reshape(1, LANES),
        first_gate,
        first_up,
    )
    heads, first = in_kernel(
        send_heads,
        (like((kv, 80, LANES), bf16), stream_like),
        hidden_sums(units, first_down),
        stream,
        mixer_gain.reshape(1, LANES),
        w_query,
        w_key,
        w_value,
    )
    rows, local, shard_heads, _ = key_cache.shape
    parts, own = pl.pallas_call(
        attend,
        out_shape=(like((kv, 16, LANES), bf16), like((16, LANES), f32)),
        in_specs=[pl.BlockSpec(memory_space=pltpu.SMEM)]
        + [pl.BlockSpec(memory_space=pltpu.VMEM)] * 3,
        out_specs=(pl.BlockSpec(memory_space=pltpu.VMEM),) * 2,
        scratch_shapes=[pltpu.VMEM((LANES, LANES), f32)],
        compiler_params=pltpu.CompilerParams(vmem_limit_bytes=32 << 20),
        name="attend",
    )(
        lengths,
        swap(heads, KV),
        key_cache.reshape(rows, local * shard_heads, LANES),
        value_cache.reshape(rows, local * shard_heads, LANES),
    )
    attended = in_kernel(
        merge,
        tile_like,
        swap(parts, KV),
        own,
        lam_heads.reshape(1, shard_heads),
        head_gain.reshape(1, LANES),
    )
    sums = swap(in_kernel(sum_heads, sums_like, swap(attended, KV), w_output), "tp")
    units, second = in_kernel(
        last_units,
        (units_like, stream_like),
        sums,
        first,
        last_gain.reshape(1, LANES),
        last_gate,
        last_up,
    )
    return in_kernel(
        finish, like((ROWS, ROWS), bf16), hidden_sums(units, last_down), second
    )


def solution(mesh):
    finer = Mesh(mesh.devices.reshape(8, 4, mesh.shape["tp"]), ("kv_0", "kv_1", "tp"))
    return jax.shard_map(
        on_device,
        mesh=finer,
        in_specs=(
            P(None, KV_TP),
            P(KV),
            P(KV, "tp"),
            P(KV, "tp"),
            P("tp", KV),
            P(KV),
            P(KV, "tp"),
            P(KV, "tp"),
            P(KV, "tp"),
            P("tp", KV),
            P("tp"),
            P(),
            P(None, KV, "tp", None),
            P(None, KV, "tp", None),
            P(),
            P(KV),
            P(KV, "tp"),
            P(KV, "tp"),
            P("tp", KV),
        ),
        out_specs=P(None, KV_TP),
        check_vma=False,
    )
```

time: 438 us -> 173 us (0.39)
  waiting for transfers between devices: 262 us -> 0 us
  blocking collectives: 97.2 us -> 151 us
  starting transfers between devices: 24.7 us -> 0 us
  between operations: 13.7 us -> 0.09 us
  matrix products: 12.4 us -> 0 us
  other arithmetic: 9.27 us -> 0 us
  Pallas kernels: 0 us -> 8.42 us
  local copies, waits for them, and re-layouts: 17.4 us -> 12.7 us
    psum x4 -> x0, waiting for transfers between devices: 234 us -> none  [one_axis_at_a_time(): return functools.reduce(lax.psum, axes, array)]
    all_to_all x6 -> x11, blocking collectives: 65.5 us -> 151 us  [swap(): return lax.all_to_all(blocks, axis, split_axis=0, concat_axis=0, tiled=True)]
    all_gather x2 -> x0, blocking collectives: 31.7 us -> none  [all_in_one(): both, at, found = (lax.all_gather(jnp.concatenate(lines), axis), 0, {})]
    all_to_all x4 -> x0, waiting for transfers between devices: 28.7 us -> none  [sent_to_all(): return lax.all_to_all(copies, axis, split_axis=0, concat_axis=0, tiled=True)]
    all_to_all x4 -> x0, starting transfers between devices: 24.5 us -> none  [sent_to_all(): return lax.all_to_all(copies, axis, split_axis=0, concat_axis=0, tiled=True)]
    dot_general x12 -> x0, matrix products: 12.4 us -> none  [the longest x1 3 us: attend(): jnp.einsum('bhmd,bphmd->bhmp', query_rows, key_entries, preferred_element...]
    pallas_call x0 -> x12, Pallas kernels: none -> 8.42 us  [the longest x1 5.65 us: on_device(): pl.pallas_call(attend, out_shape=(like((kv, 16, LANES), bf16), like((16,...]
  transfers between devices with their start and end apart: 8 -> 0, of which waited for: 7 -> 0; matrix products, arithmetic and copies ran while one was open for 4% -> 0% of each run, Pallas kernels for 0% -> 0%
where the time goes in v1:
time: 173 us; the launch traced here: 172 us
  blocking collectives  151 us (87%)
  local copies, waits for them, and re-layouts  12.7 us (7%)
  Pallas kernels  8.42 us (5%)
    all_to_all x11, blocking collectives, swap(): return lax.all_to_all(blocks, axis, split_axis=0, concat_axis=0, tiled=True)  151 us
    unnamed x38, local copies, waits for them, and re-layouts  12.7 us
    pallas_call x1, Pallas kernels, on_device(): pl.pallas_call(attend, out_shape=(like((kv, 16, LANES), bf16), like((16,...  5.65 us

profile of v1, /device:TPU:1, one launch (start us, length us, event | category | flops | bytes accessed | tf_op | source)
XLA Modules:
  0.0 172.0 jit_solution(9817970405305284288)
XLA Ops:
  0.0 0.0 copy-start.12
  0.0 0.7 copy-done.12
  0.7 0.1 spread_tokens.1
  0.8 10.3 %all_to_all.55.blocks_ref = bf16[8,16,128]{2,1,0:T(8,128)(2,1)S(1)} all-to-all(bf16[8,16,128]{2,1,0:T(8,128)(2,1)S(1)} %spread_tokens.1), channel_id=1, replica_groups=mesh['kv_0'=8,'kv_1'=4,'tp'=8] {'tp'}, dimensions={0} | all-to-all | bytes 65536 | tf_op jit(solution)/shard_map/all_to_all | solution.py:45
  11.1 0.0 copy-start.2
  11.1 1.0 copy-done.2
  12.1 0.0 copy-start.3
  12.1 1.0 copy-done.3
  13.1 0.7 copy-done.13
  13.7 0.2 first_units.1
  13.9 21.1 %all_to_all.56.parts_ref = bf16[32,24,128]{2,1,0:T(8,128)(2,1)S(1)} all-to-all(bf16[32,24,128]{2,1,0:T(8,128)(2,1)S(1)} %get-tuple-element.13), channel_id=1, replica_groups=mesh['kv_0'=8,'kv_1'=4,'tp'=8] {'kv_0','kv_1'}, dimensions={0} | all-to-all | bytes 393216 | tf_op jit(solution)/shard_map/all_to_all | solution.py:45
  35.0 0.1 gate_units.2
  35.1 13.3 %all_to_all.57.hidden_ref = bf16[32,8,128]{2,1,0:T(8,128)(2,1)S(1)} all-to-all(bf16[32,8,128]{2,1,0:T(8,128)(2,1)S(1)} %gate_units.2), channel_id=1, replica_groups=mesh['kv_0'=8,'kv_1'=4,'tp'=8] {'kv_0','kv_1'}, dimensions={0} | all-to-all | bytes 131072 | tf_op jit(solution)/shard_map/all_to_all | solution.py:45
  48.4 1.0 copy-done.6
  49.4 0.2 sum_down.2
  49.5 10.0 %all_to_all.58.blocks_ref = f32[8,16,128]{2,1,0:T(8,128)S(1)} all-to-all(f32[8,16,128]{2,1,0:T(8,128)S(1)} %sum_down.2), channel_id=1, replica_groups=mesh['kv_0'=8,'kv_1'=4,'tp'=8] {'tp'}, dimensions={0} | all-to-all | bytes 131072 | tf_op jit(solution)/shard_map/all_to_all | solution.py:45
  59.6 0.9 copy-done.8
  60.5 0.9 copy-done.9
  61.4 0.9 copy-done.10
  62.3 0.7 copy-done.17
  62.9 0.3 send_heads.1
  63.3 21.9 %all_to_all.59.parts_ref = bf16[32,80,128]{2,1,0:T(8,128)(2,1)S(1)} all-to-all(bf16[32,80,128]{2,1,0:T(8,128)(2,1)S(1)} %get-tuple-element.15), channel_id=1, replica_groups=mesh['kv_0'=8,'kv_1'=4,'tp'=8] {'kv_0','kv_1'}, dimensions={0} | all-to-all | bytes 1310720 | tf_op jit(solution)/shard_map/all_to_all | solution.py:45
  85.2 2.2 %copy-done = bf16[16,256,4,128]{3,2,1,0:T(4,128)(2,1)S(1)} copy-done((bf16[16,256,4,128]{3,2,1,0:T(4,128)(2,1)S(1)}, bf16[16,256,4,128]{3,2,1,0:T(4,128)(2,1)}, u32[]{:S(2)}) %copy-start) | copy-done | bytes 4194328
  87.4 2.2 %copy-done.1 = bf16[16,256,4,128]{3,2,1,0:T(4,128)(2,1)S(1)} copy-done((bf16[16,256,4,128]{3,2,1,0:T(4,128)(2,1)S(1)}, bf16[16,256,4,128]{3,2,1,0:T(4,128)(2,1)}, u32[]{:S(2)}) %copy-start.1) | copy-done | bytes 4194328
  89.6 0.7 copy-done.14
  90.2 0.0 copy-start.5
  90.2 0.0 copy-start.18
  90.2 0.0 copy-start.7
  90.3 5.6 %attend.1 = (bf16[32,16,128]{2,1,0:T(8,128)(2,1)S(1)}, f32[16,128]{1,0:T(8,128)S(1)}) custom-call(s32[16]{0:T(128)S(1)} %copy-done.14, bf16[32,80,128]{2,1,0:T(8,128)(2,1)S(1)} %all_to_all.59.parts_ref, bf16[16,1024,128]{2,1,0:T(8,128)(2,1)S(1)} %bitcast.7, bf16[16,1024,128]{2,1,0:T(8,128)(2,1)S(1)} %bitcast.8), custom_call_target="tpu_custom_call" | custom-call | tf_op jit(solution)/shard_map/attend/pallas_call | solution.py:319
  95.9 14.4 %all_to_all.60.parts_ref = bf16[32,16,128]{2,1,0:T(8,128)(2,1)S(1)} all-to-all(bf16[32,16,128]{2,1,0:T(8,128)(2,1)S(1)} %get-tuple-element.16), channel_id=1, replica_groups=mesh['kv_0'=8,'kv_1'=4,'tp'=8] {'kv_0','kv_1'}, dimensions={0} | all-to-all | bytes 262144 | tf_op jit(solution)/shard_map/all_to_all | solution.py:45
  110.3 0.0 copy-done.15
  110.3 0.0 copy-done.16
  110.3 0.4 merge.1
  110.7 12.1 %all_to_all.61.attended_ref = bf16[32,8,128]{2,1,0:T(8,128)(2,1)S(1)} all-to-all(bf16[32,8,128]{2,1,0:T(8,128)(2,1)S(1)} %merge.1), channel_id=1, replica_groups=mesh['kv_0'=8,'kv_1'=4,'tp'=8] {'kv_0','kv_1'}, dimensions={0} | all-to-all | bytes 131072 | tf_op jit(solution)/shard_map/all_to_all | solution.py:45
  122.8 0.0 copy-done.11
  122.8 0.2 sum_heads.1
  123.1 11.5 %all_to_all.62.blocks_ref = f32[8,16,128]{2,1,0:T(8,128)S(1)} all-to-all(f32[8,16,128]{2,1,0:T(8,128)S(1)} %sum_heads.1), channel_id=1, replica_groups=mesh['kv_0'=8,'kv_1'=4,'tp'=8] {'tp'}, dimensions={0} | all-to-all | bytes 131072 | tf_op jit(solution)/shard_map/all_to_all | solution.py:45
  134.5 0.0 copy-done.4
  134.5 0.0 copy-done.5
  134.5 0.0 copy-done.18
  134.5 0.2 last_units.1
  134.7 13.0 %all_to_all.63.parts_ref = bf16[32,24,128]{2,1,0:T(8,128)(2,1)S(1)} all-to-all(bf16[32,24,128]{2,1,0:T(8,128)(2,1)S(1)} %get-tuple-element.19), channel_id=1, replica_groups=mesh['kv_0'=8,'kv_1'=4,'tp'=8] {'kv_0','kv_1'}, dimensions={0} | all-to-all | bytes 393216 | tf_op jit(solution)/shard_map/all_to_all | solution.py:45
  147.7 0.1 gate_units.3
  147.9 13.1 %all_to_all.64.hidden_ref = bf16[32,8,128]{2,1,0:T(8,128)(2,1)S(1)} all-to-all(bf16[32,8,128]{2,1,0:T(8,128)(2,1)S(1)} %gate_units.3), channel_id=1, replica_groups=mesh['kv_0'=8,'kv_1'=4,'tp'=8] {'kv_0','kv_1'}, dimensions={0} | all-to-all | bytes 131072 | tf_op jit(solution)/shard_map/all_to_all | solution.py:45
  160.9 0.0 copy-done.7
  160.9 0.2 sum_down.3
  161.1 10.2 %all_to_all.65.blocks_ref = f32[8,16,128]{2,1,0:T(8,128)S(1)} all-to-all(f32[8,16,128]{2,1,0:T(8,128)S(1)} %sum_down.3), channel_id=1, replica_groups=mesh['kv_0'=8,'kv_1'=4,'tp'=8] {'tp'}, dimensions={0} | all-to-all | bytes 131072 | tf_op jit(solution)/shard_map/all_to_all | solution.py:45
  171.3 0.7 finish.1
  (13 shorter events, 0.0 us)
Async XLA Ops:
  0.0 0.7 copy-start.12
  11.1 1.0 copy-start.2
  12.1 1.0 copy-start.3
  13.1 0.7 copy-start.13
  48.4 1.0 copy-start.6
  59.6 0.9 copy-start.8
  60.5 0.9 copy-start.9
  61.4 0.9 copy-start.10
  62.3 0.7 copy-start.17
  85.2 2.2 %copy-start = (bf16[16,256,4,128]{3,2,1,0:T(4,128)(2,1)S(1)}, bf16[16,256,4,128]{3,2,1,0:T(4,128)(2,1)}, u32[]{:S(2)}) copy-start(bf16[16,256,4,128]{3,2,1,0:T(4,128)(2,1)} %param.31) | copy-start | bytes 12582916
  87.4 2.2 %copy-start.1 = (bf16[16,256,4,128]{3,2,1,0:T(4,128)(2,1)S(1)}, bf16[16,256,4,128]{3,2,1,0:T(4,128)(2,1)}, u32[]{:S(2)}) copy-start(bf16[16,256,4,128]{3,2,1,0:T(4,128)(2,1)} %param.32) | copy-start | bytes 12582916
  89.6 0.7 copy-start.14
  90.2 20.1 %copy-start.15 = (f32[4]{0:T(128)S(1)}, f32[4]{0:T(128)}, u32[]{:S(2)}) copy-start(f32[4]{0:T(128)} %param.29) | copy-start | bytes 52
  90.2 20.1 %copy-start.16 = (f32[128]{0:T(128)S(1)}, f32[128]{0:T(128)}, u32[]{:S(2)}) copy-start(f32[128]{0:T(128)} %param.30) | copy-start | bytes 1540
  90.2 32.6 %copy-start.11 = (bf16[512,128]{1,0:T(8,128)(2,1)S(1)}, bf16[512,128]{1,0:T(8,128)(2,1)}, u32[]{:S(2)}) copy-start(bf16[512,128]{1,0:T(8,128)(2,1)} %weight_ref.1) | copy-start | bytes 393220
  90.2 44.3 %copy-start.4 = (bf16[128,1408]{1,0:T(8,128)(2,1)S(1)}, bf16[128,1408]{1,0:T(8,128)(2,1)}, u32[]{:S(2)}) copy-start(bf16[128,1408]{1,0:T(8,128)(2,1)} %gate_ref.3) | copy-start | bytes 1081348
  90.2 44.3 %copy-start.5 = (bf16[128,1408]{1,0:T(8,128)(2,1)S(1)}, bf16[128,1408]{1,0:T(8,128)(2,1)}, u32[]{:S(2)}) copy-start(bf16[128,1408]{1,0:T(8,128)(2,1)} %up_ref.3) | copy-start | bytes 1081348
  90.2 44.3 %copy-start.18 = (f32[128]{0:T(128)S(1)}, f32[128]{0:T(128)}, u32[]{:S(2)}) copy-start(f32[128]{0:T(128)} %param.34) | copy-start | bytes 1540
  90.2 70.7 %copy-start.7 = (bf16[1408,128]{1,0:T(8,128)(2,1)S(1)}, bf16[1408,128]{1,0:T(8,128)(2,1)}, u32[]{:S(2)}) copy-start(bf16[1408,128]{1,0:T(8,128)(2,1)} %down_ref.3) | copy-start | bytes 1081348

commit v2 on v1

--- a/solution.py
+++ b/solution.py
@@ -19,6 +19,7 @@
 neg_fill = -1e30
 f32 = jnp.float32
 bf16 = jnp.bfloat16
+covering = pl.CostEstimate(flops=10**10, bytes_accessed=10**5, transcendentals=0)
 
 
 def iota(shape, dim):
@@ -37,6 +38,7 @@
         in_specs=[pl.BlockSpec(memory_space=space) for space in spaces],
         out_specs=jax.tree.map(lambda _: pl.BlockSpec(memory_space=pltpu.VMEM), outs),
         compiler_params=pltpu.CompilerParams(vmem_limit_bytes=vmem_limit),
+        cost_estimate=covering,
         name=body.__name__,
     )(*args)
 
@@ -324,6 +326,7 @@
         out_specs=(pl.BlockSpec(memory_space=pltpu.VMEM),) * 2,
         scratch_shapes=[pltpu.VMEM((LANES, LANES), f32)],
         compiler_params=pltpu.CompilerParams(vmem_limit_bytes=32 << 20),
+        cost_estimate=covering,
         name="attend",
     )(
         lengths,

time: 173 us -> 161 us (0.931)
  local copies, waits for them, and re-layouts: 12.7 us -> 0.84 us
    unnamed x38, local copies, waits for them, and re-layouts: 12.7 us -> 0.84 us
where the time goes in v2:
time: 161 us
  blocking collectives  151 us (94%)
  Pallas kernels  8.43 us (5%)
    all_to_all x11, blocking collectives, swap(): return lax.all_to_all(blocks, axis, split_axis=0, concat_axis=0, tiled=True)  151 us
    pallas_call x1, Pallas kernels, on_device(): pl.pallas_call(attend, out_shape=(like((kv, 16, LANES), bf16), like((16,...  5.65 us

profile of v2, /device:TPU:1, one launch (start us, length us, event | category | flops | bytes accessed | tf_op | source)
XLA Modules:
  0.0 160.7 jit_solution(12772572571186513033)
XLA Ops:
  0.0 0.8 copy-done.12
  0.8 0.1 spread_tokens.1
  0.9 10.3 %all_to_all.55.blocks_ref = bf16[8,16,128]{2,1,0:T(8,128)(2,1)S(1)} all-to-all(bf16[8,16,128]{2,1,0:T(8,128)(2,1)S(1)} %spread_tokens.1), channel_id=1, replica_groups=mesh['kv_0'=8,'kv_1'=4,'tp'=8] {'tp'}, dimensions={0} | all-to-all | bytes 65536 | tf_op jit(solution)/shard_map/all_to_all | solution.py:47
  11.2 0.0 copy-done.3
  11.2 0.0 copy-done.2
  11.2 0.0 copy-done.13
  11.2 0.2 first_units.1
  11.4 21.1 %all_to_all.56.parts_ref = bf16[32,24,128]{2,1,0:T(8,128)(2,1)S(1)} all-to-all(bf16[32,24,128]{2,1,0:T(8,128)(2,1)S(1)} %get-tuple-element.13), channel_id=1, replica_groups=mesh['kv_0'=8,'kv_1'=4,'tp'=8] {'kv_0','kv_1'}, dimensions={0} | all-to-all | bytes 393216 | tf_op jit(solution)/shard_map/all_to_all | solution.py:47
  32.5 0.1 gate_units.2
  32.6 13.3 %all_to_all.57.hidden_ref = bf16[32,8,128]{2,1,0:T(8,128)(2,1)S(1)} all-to-all(bf16[32,8,128]{2,1,0:T(8,128)(2,1)S(1)} %gate_units.2), channel_id=1, replica_groups=mesh['kv_0'=8,'kv_1'=4,'tp'=8] {'kv_0','kv_1'}, dimensions={0} | all-to-all | bytes 131072 | tf_op jit(solution)/shard_map/all_to_all | solution.py:47
  45.8 0.0 copy-done.4
  45.9 0.0 copy-start.14
  45.9 0.2 sum_down.2
  46.0 10.2 %all_to_all.58.blocks_ref = f32[8,16,128]{2,1,0:T(8,128)S(1)} all-to-all(f32[8,16,128]{2,1,0:T(8,128)S(1)} %sum_down.2), channel_id=1, replica_groups=mesh['kv_0'=8,'kv_1'=4,'tp'=8] {'tp'}, dimensions={0} | all-to-all | bytes 131072 | tf_op jit(solution)/shard_map/all_to_all | solution.py:47
  56.2 0.0 copy-done.8
  56.2 0.0 copy-done.9
  56.2 0.0 copy-done.10
  56.2 0.0 copy-done.14
  56.2 0.0 copy-start
  56.2 0.0 copy-start.1
  56.2 0.0 copy-start.15
  56.3 0.3 send_heads.1
  56.6 22.3 %all_to_all.59.parts_ref = bf16[32,80,128]{2,1,0:T(8,128)(2,1)S(1)} all-to-all(bf16[32,80,128]{2,1,0:T(8,128)(2,1)S(1)} %get-tuple-element.15), channel_id=1, replica_groups=mesh['kv_0'=8,'kv_1'=4,'tp'=8] {'kv_0','kv_1'}, dimensions={0} | all-to-all | bytes 1310720 | tf_op jit(solution)/shard_map/all_to_all | solution.py:47
  78.9 0.0 copy-done
  78.9 0.0 copy-done.1
  78.9 0.0 copy-done.15
  78.9 0.0 copy-start.16
  78.9 0.0 copy-start.17
  78.9 5.6 %attend.1 = (bf16[32,16,128]{2,1,0:T(8,128)(2,1)S(1)}, f32[16,128]{1,0:T(8,128)S(1)}) custom-call(s32[16]{0:T(128)S(1)} %copy-done.15, bf16[32,80,128]{2,1,0:T(8,128)(2,1)S(1)} %all_to_all.59.parts_ref, bf16[16,1024,128]{2,1,0:T(8,128)(2,1)S(1)} %bitcast.7, bf16[16,1024,128]{2,1,0:T(8,128)(2,1)S(1)} %bitcast.8), custom_call_target="tpu_custom_call" | custom-call | flops 10000000000 | bytes 100000 | tf_op jit(solution)/shard_map/attend/pallas_call | solution.py:321
  84.6 14.5 %all_to_all.60.parts_ref = bf16[32,16,128]{2,1,0:T(8,128)(2,1)S(1)} all-to-all(bf16[32,16,128]{2,1,0:T(8,128)(2,1)S(1)} %get-tuple-element.16), channel_id=1, replica_groups=mesh['kv_0'=8,'kv_1'=4,'tp'=8] {'kv_0','kv_1'}, dimensions={0} | all-to-all | bytes 262144 | tf_op jit(solution)/shard_map/all_to_all | solution.py:47
  99.0 0.0 copy-done.16
  99.0 0.0 copy-done.17
  99.1 0.4 merge.1
  99.5 12.1 %all_to_all.61.attended_ref = bf16[32,8,128]{2,1,0:T(8,128)(2,1)S(1)} all-to-all(bf16[32,8,128]{2,1,0:T(8,128)(2,1)S(1)} %merge.1), channel_id=1, replica_groups=mesh['kv_0'=8,'kv_1'=4,'tp'=8] {'kv_0','kv_1'}, dimensions={0} | all-to-all | bytes 131072 | tf_op jit(solution)/shard_map/all_to_all | solution.py:47
  111.6 0.0 copy-done.11
  111.6 0.2 sum_heads.1
  111.8 11.4 %all_to_all.62.blocks_ref = f32[8,16,128]{2,1,0:T(8,128)S(1)} all-to-all(f32[8,16,128]{2,1,0:T(8,128)S(1)} %sum_heads.1), channel_id=1, replica_groups=mesh['kv_0'=8,'kv_1'=4,'tp'=8] {'tp'}, dimensions={0} | all-to-all | bytes 131072 | tf_op jit(solution)/shard_map/all_to_all | solution.py:47
  123.2 0.0 copy-done.5
  123.2 0.0 copy-done.6
  123.2 0.0 copy-done.18
  123.2 0.2 last_units.1
  123.4 13.0 %all_to_all.63.parts_ref = bf16[32,24,128]{2,1,0:T(8,128)(2,1)S(1)} all-to-all(bf16[32,24,128]{2,1,0:T(8,128)(2,1)S(1)} %get-tuple-element.19), channel_id=1, replica_groups=mesh['kv_0'=8,'kv_1'=4,'tp'=8] {'kv_0','kv_1'}, dimensions={0} | all-to-all | bytes 393216 | tf_op jit(solution)/shard_map/all_to_all | solution.py:47
  136.4 0.1 gate_units.3
  136.6 13.1 %all_to_all.64.hidden_ref = bf16[32,8,128]{2,1,0:T(8,128)(2,1)S(1)} all-to-all(bf16[32,8,128]{2,1,0:T(8,128)(2,1)S(1)} %gate_units.3), channel_id=1, replica_groups=mesh['kv_0'=8,'kv_1'=4,'tp'=8] {'kv_0','kv_1'}, dimensions={0} | all-to-all | bytes 131072 | tf_op jit(solution)/shard_map/all_to_all | solution.py:47
  149.6 0.0 copy-done.7
  149.6 0.2 sum_down.3
  149.8 10.2 %all_to_all.65.blocks_ref = f32[8,16,128]{2,1,0:T(8,128)S(1)} all-to-all(f32[8,16,128]{2,1,0:T(8,128)S(1)} %sum_down.3), channel_id=1, replica_groups=mesh['kv_0'=8,'kv_1'=4,'tp'=8] {'tp'}, dimensions={0} | all-to-all | bytes 131072 | tf_op jit(solution)/shard_map/all_to_all | solution.py:47
  160.0 0.7 finish.1
  (13 shorter events, 0.0 us)
Async XLA Ops:
  0.0 11.2 %copy-start.3 = (bf16[128,1408]{1,0:T(8,128)(2,1)S(1)}, bf16[128,1408]{1,0:T(8,128)(2,1)}, u32[]{:S(2)}) copy-start(bf16[128,1408]{1,0:T(8,128)(2,1)} %up_ref.2) | copy-start | bytes 1081348
  0.0 11.2 %copy-start.2 = (bf16[128,1408]{1,0:T(8,128)(2,1)S(1)}, bf16[128,1408]{1,0:T(8,128)(2,1)}, u32[]{:S(2)}) copy-start(bf16[128,1408]{1,0:T(8,128)(2,1)} %gate_ref.2) | copy-start | bytes 1081348
  0.0 0.8 copy-start.12
  0.8 10.4 %copy-start.13 = (f32[128]{0:T(128)S(1)}, f32[128]{0:T(128)}, u32[]{:S(2)}) copy-start(f32[128]{0:T(128)} %param.20) | copy-start | bytes 1540
  32.4 13.4 %copy-start.4 = (bf16[1408,128]{1,0:T(8,128)(2,1)S(1)}, bf16[1408,128]{1,0:T(8,128)(2,1)}, u32[]{:S(2)}) copy-start(bf16[1408,128]{1,0:T(8,128)(2,1)} %down_ref.2) | copy-start | bytes 1081348
  45.8 10.4 %copy-start.8 = (bf16[128,512]{1,0:T(8,128)(2,1)S(1)}, bf16[128,512]{1,0:T(8,128)(2,1)}, u32[]{:S(2)}) copy-start(bf16[128,512]{1,0:T(8,128)(2,1)} %query_ref.1) | copy-start | bytes 393220
  45.8 10.4 %copy-start.9 = (bf16[128,512]{1,0:T(8,128)(2,1)S(1)}, bf16[128,512]{1,0:T(8,128)(2,1)}, u32[]{:S(2)}) copy-start(bf16[128,512]{1,0:T(8,128)(2,1)} %key_ref.1) | copy-start | bytes 393220
  45.9 10.4 %copy-start.10 = (bf16[128,512]{1,0:T(8,128)(2,1)S(1)}, bf16[128,512]{1,0:T(8,128)(2,1)}, u32[]{:S(2)}) copy-start(bf16[128,512]{1,0:T(8,128)(2,1)} %value_ref.1) | copy-start | bytes 393220
  45.9 10.4 %copy-start.14 = (f32[128]{0:T(128)S(1)}, f32[128]{0:T(128)}, u32[]{:S(2)}) copy-start(f32[128]{0:T(128)} %param.24) | copy-start | bytes 1540
  56.2 22.7 %copy-start = (bf16[16,256,4,128]{3,2,1,0:T(4,128)(2,1)S(1)}, bf16[16,256,4,128]{3,2,1,0:T(4,128)(2,1)}, u32[]{:S(2)}) copy-start(bf16[16,256,4,128]{3,2,1,0:T(4,128)(2,1)} %param.31) | copy-start | bytes 12582916
  56.2 22.7 %copy-start.1 = (bf16[16,256,4,128]{3,2,1,0:T(4,128)(2,1)S(1)}, bf16[16,256,4,128]{3,2,1,0:T(4,128)(2,1)}, u32[]{:S(2)}) copy-start(bf16[16,256,4,128]{3,2,1,0:T(4,128)(2,1)} %param.32) | copy-start | bytes 12582916
  56.2 22.7 %copy-start.15 = (s32[16]{0:T(128)S(1)}, s32[16]{0:T(128)}, u32[]{:S(2)}) copy-start(s32[16]{0:T(128)} %lengths_ref.1) | copy-start | bytes 196
  78.9 20.1 %copy-start.16 = (f32[4]{0:T(128)S(1)}, f32[4]{0:T(128)}, u32[]{:S(2)}) copy-start(f32[4]{0:T(128)} %param.29) | copy-start | bytes 52
  78.9 20.1 %copy-start.17 = (f32[128]{0:T(128)S(1)}, f32[128]{0:T(128)}, u32[]{:S(2)}) copy-start(f32[128]{0:T(128)} %param.30) | copy-start | bytes 1540
  99.1 12.5 %copy-start.11 = (bf16[512,128]{1,0:T(8,128)(2,1)S(1)}, bf16[512,128]{1,0:T(8,128)(2,1)}, u32[]{:S(2)}) copy-start(bf16[512,128]{1,0:T(8,128)(2,1)} %weight_ref.1) | copy-start | bytes 393220
  111.6 11.7 %copy-start.5 = (bf16[128,1408]{1,0:T(8,128)(2,1)S(1)}, bf16[128,1408]{1,0:T(8,128)(2,1)}, u32[]{:S(2)}) copy-start(bf16[128,1408]{1,0:T(8,128)(2,1)} %gate_ref.3) | copy-start | bytes 1081348
  111.6 11.7 %copy-start.6 = (bf16[128,1408]{1,0:T(8,128)(2,1)S(1)}, bf16[128,1408]{1,0:T(8,128)(2,1)}, u32[]{:S(2)}) copy-start(bf16[128,1408]{1,0:T(8,128)(2,1)} %up_ref.3) | copy-start | bytes 1081348
  111.6 11.7 %copy-start.18 = (f32[128]{0:T(128)S(1)}, f32[128]{0:T(128)}, u32[]{:S(2)}) copy-start(f32[128]{0:T(128)} %param.34) | copy-start | bytes 1540
  136.4 13.2 %copy-start.7 = (bf16[1408,128]{1,0:T(8,128)(2,1)S(1)}, bf16[1408,128]{1,0:T(8,128)(2,1)}, u32[]{:S(2)}) copy-start(bf16[1408,128]{1,0:T(8,128)(2,1)} %down_ref.3) | copy-start | bytes 1081348
